TPU v7x, 32 devices: a whole 2x2x4 slice. The times are simulated.
32 devices in a mesh: grp: 2 (over y), sp: 4 (over z), tp: 4 (over x, core).
Axes of the slice: x: 2, y: 2, z: 4, core: 2. Of those that a mesh axis runs over, the one named last changes fastest.
Arguments:
- hidden_in: bfloat16 [5120, 4096], P(('grp', 'sp'), 'tp'), parts along dimension 0, may hold values from -64 to 64
- norm_gain: float32 [2, 4096], replicated, may hold values from 0.1 to 1.9
- w_pool_in: bfloat16 [2, 4096, 1024], P(None, 'sp', 'tp'), may hold values from -0.09375 to 0.09375
- w_pool_gate: bfloat16 [2, 4096, 1024], P(None, 'sp', 'tp'), may hold values from -0.09375 to 0.09375
- group_mix: bfloat16 [2, 16, 64, 64], replicated, may hold values from -0.75 to 0.75
- w_out: bfloat16 [2, 1024, 4096], P(None, 'sp', 'tp'), may hold values from -0.1875 to 0.1875
Outputs:
- hidden_out: bfloat16 [5120, 4096], P(('grp', 'sp'), 'tp'), parts along dimension 0
There are 2 independent parts, one for each index of `grp`. A program takes and returns all parts, laid end to end along the dimension named above; an argument that names none is the same for every part. Nothing has to cross between parts.
All inputs are finite; a program needn't handle non-finite values.
Results may differ from a plain program's by a relative error of at most 0.012.
Values may be sent and summed in bfloat16 or wider, within the bound.
A program may use at most 64 MiB of HBM per device.

v0:
```python
import functools

import jax
import jax.numpy as jnp
from jax import lax
from jax.experimental import pallas as pl
from jax.experimental.pallas import tpu as pltpu
from jax.sharding import PartitionSpec as P

GROUP = 64
HALO = 8
SUBS = 1
AHEAD = 2
START = (0.0, 0.34)
GATHERED = (0.56, 0.67)
PROJECTED = (0.78, 0.89)
GATED = (0.89, 1.0)
POOLED = (1.0, 1.23)
RELAYED = (1.0, 1.23)
MESH = pl.DeviceIdType.MESH

norm_eps = 1e-06


def mixer(dims, h_in, gain, w_in, w_gate, mix, w_out, out, hg, nb, br, wi, wg, wo, pad, acc_p, acc_g, bd,
          local_sem, zr, zs, yr, ys, gr, gs, pr, ps):
    sp_size, tp_size, layers, rows, cols, chans, chunks = dims
    step_rows = rows // chunks
    chips = tp_size // 2
    half = lax.axis_index("grp")
    row_rank = lax.axis_index("sp")
    rank = lax.axis_index("tp")
    chip, core = rank // 2, lax.rem(rank, 2)
    sibling = chip * 2 + 1 - core
    other = 1 - half
    total_rows = rows * sp_size
    shards = ((w_in, wi), (w_gate, wg), (w_out, wo))

    def chip_rank(distance):
        return lax.rem(chip + distance, chips) * 2 + core

    own_w = []
    for layer in range(layers):
        for t, (shard, whole) in enumerate(shards):
            depth = shard.shape[1]
            copy = pltpu.make_async_copy(
                shard.at[layer],
                whole.at[layer, pl.ds(pl.multiple_of(row_rank * depth, depth), depth)],
                local_sem.at[1 + layer * 3 + t],
            )
            copy.start()
            own_w.append(copy)
    own_h = pltpu.make_async_copy(h_in, hg.at[0, rank], local_sem.at[0])
    own_h.start()

    barrier = pltpu.get_barrier_semaphore()
    peers = [
        {"sp": lax.rem(row_rank + 1, sp_size)},
        {"sp": lax.rem(row_rank + sp_size - 1, sp_size)},
        {"grp": other},
        {"tp": sibling},
    ] + [{"tp": chip_rank(d)} for d in range(1, chips)]
    for peer in peers:
        pl.semaphore_signal(barrier, inc=1, device_id=peer, device_id_type=MESH)
    pl.semaphore_wait(barrier, len(peers))

    pieces = [(layer, t, sub) for layer in range(layers) for t in range(3) for sub in range(SUBS)]
    final = len(pieces) - 1
    extra = final + 1
    pieces.append(pieces[final])
    ends = (0, sp_size - 1)

    def swapped(q, source):
        return q < final or (q == final and source not in ends)

    def piece_ref(q, source, part):
        layer, t, sub = pieces[q]
        shard, whole = shards[t]
        depth = shard.shape[1]
        size = depth // (2 * SUBS)
        start = pl.multiple_of(source * depth + (part * SUBS + sub) * size, size)
        return whole.at[layer, pl.ds(start, size)]

    def z_copy(q, source, to, send):
        ref = piece_ref(q, source, other if q == extra else half)
        return pltpu.make_async_remote_copy(
            ref, ref, zs.at[q, send], zr.at[q, source], device_id={"sp": to}, device_id_type=MESH
        )

    def y_copy(q, source, part):
        ref = piece_ref(q, source, part)
        return pltpu.make_async_remote_copy(
            ref, ref, ys.at[q, source], yr.at[q, source], device_id={"grp": other}, device_id_type=MESH
        )

    up = jnp.minimum(row_rank + 1, sp_size - 1)
    down = jnp.maximum(row_rank - 1, 0)

    def z_own(q):
        layer, t, sub = pieces[q]
        if sub == 0 and q < extra:
            own_w[layer * 3 + t].wait()

        @pl.when((row_rank == 0) if q == extra else (row_rank < sp_size - 1))
        def _():
            z_copy(q, row_rank, up, row_rank).start()

        @pl.when((row_rank == sp_size - 1) if q == extra else (row_rank > 0))
        def _():
            z_copy(q, row_rank, down, sp_size).start()

    def z_step(q, distance):
        low, high = row_rank - distance, row_rank + distance

        @pl.when((low == 0) if q == extra else (low >= 0))
        def _():
            z_copy(q, low, up, low).wait_recv()

            @pl.when(row_rank < sp_size - 1)
            def _():
                z_copy(q, low, up, low).start()

            if q < final:
                y_copy(q, low, half).start()
            elif q == final:
                @pl.when(low > 0)
                def _():
                    y_copy(q, low, half).start()

        @pl.when((high == sp_size - 1) if q == extra else (high < sp_size))
        def _():
            z_copy(q, high, down, high).wait_recv()

            @pl.when(row_rank > 0)
            def _():
                z_copy(q, high, down, high).start()

            if q < final:
                y_copy(q, high, half).start()
            elif q == final:
                @pl.when(high < sp_size - 1)
                def _():
                    y_copy(q, high, half).start()

        if distance == sp_size - 1 and q + AHEAD < len(pieces):
            z_own(q + AHEAD)

    steps = [functools.partial(z_step, q, d) for q in range(len(pieces)) for d in range(1, sp_size)]

    def advance(upto):
        while steps and len(pieces) * (sp_size - 1) - len(steps) < upto:
            steps.pop(0)()

    def y_arrived(layer, t):
        for q, piece in enumerate(pieces):
            if piece[:2] == (layer, t):
                advance((q + 1) * (sp_size - 1))
                for source in range(sp_size):
                    if not swapped(q, source):
                        continue

                    @pl.when(row_rank != source)
                    def _():
                        y_copy(q, source, other).wait_recv()

    def weights_sent():
        for q in range(len(pieces)):
            for source in range(sp_size):
                if swapped(q, source):
                    @pl.when(row_rank != source)
                    def _():
                        y_copy(q, source, half).wait_send()

                if q < extra or source == 0:
                    @pl.when((source <= row_rank) & (row_rank < sp_size - 1))
                    def _():
                        z_copy(q, source, up, source).wait_send()

                if q < extra or source == sp_size - 1:
                    @pl.when((source > row_rank) & (row_rank > 0))
                    def _():
                        z_copy(q, source, down, source).wait_send()

            @pl.when((row_rank == sp_size - 1) if q == extra else (row_rank > 0))
            def _():
                z_copy(q, row_rank, down, sp_size).wait_send()

    def g_copy(kind, layer, chunk, source, to, send):
        buffer = (hg, br)[kind]
        ref = buffer.at[layer, source, pl.ds(chunk * step_rows, step_rows)]
        index = (kind * layers + layer) * chunks + chunk
        return pltpu.make_async_remote_copy(
            ref, ref, gs.at[index, send], gr.at[index, source], device_id={"tp": to}, device_id_type=MESH
        )

    def g_send(kind, layer, chunk):
        for d in range(1, chips):
            g_copy(kind, layer, chunk, rank, chip_rank(d), d).start()
        g_copy(kind, layer, chunk, rank, sibling, 0).start()

    def g_relay(kind, layer, chunk):
        for d in range(1, chips):
            source = chip_rank(d)
            g_copy(kind, layer, chunk, source, sibling, chips + d - 1).wait_recv()
            g_copy(kind, layer, chunk, source, sibling, chips + d - 1).start()

    def g_arrived(kind, layer, chunk):
        for d in range(chips):
            source = lax.rem(chip + d, chips) * 2 + 1 - core
            g_copy(kind, layer, chunk, source, sibling, 0).wait_recv()

    def g_sent(kind, layer, chunk):
        for d in range(1, chips):
            g_copy(kind, layer, chunk, rank, chip_rank(d), d).wait_send()
            g_copy(kind, layer, chunk, chip_rank(d), sibling, chips + d - 1).wait_send()
        g_copy(kind, layer, chunk, rank, sibling, 0).wait_send()

    def normalize(layer, chunk):
        span = pl.ds(chunk * step_rows, step_rows)
        squares = jnp.zeros((step_rows, 1), jnp.float32)
        for k in range(tp_size):
            block = hg[layer, k, span, :].astype(jnp.float32)
            squares = squares + jnp.sum(block * block, axis=1, keepdims=True)
        scaling = lax.rsqrt(squares / (cols * tp_size) + norm_eps)
        for k in range(tp_size):
            block = hg[layer, k, span, :].astype(jnp.float32)
            own_gain = gain[layer : layer + 1, k * cols : (k + 1) * cols]
            nb[k, span, :] = (block * scaling * own_gain).astype(jnp.bfloat16)

    def project(acc, whole, layer):
        acc[...] = jnp.zeros_like(acc)

        @pl.loop(0, tp_size)
        def _(k):
            weight = whole[layer, pl.ds(pl.multiple_of(k * cols, cols), cols), :]
            acc[...] += jnp.dot(nb[k], weight, preferred_element_type=jnp.float32)

    def halo_copy(layer, upward):
        source, target = (rows, 0) if upward else (HALO, rows + HALO)
        side = 0 if upward else 1
        return pltpu.make_async_remote_copy(
            pad.at[layer, pl.ds(source, HALO)], pad.at[layer, pl.ds(target, HALO)],
            ps.at[layer, side], pr.at[layer, side],
            device_id={"sp": up if upward else down}, device_id_type=MESH,
        )

    def halo_send(layer):
        @pl.when(row_rank < sp_size - 1)
        def _():
            halo_copy(layer, True).start()

        @pl.when(row_rank > 0)
        def _():
            halo_copy(layer, False).start()

    def halo_arrived(layer):
        @pl.when(row_rank > 0)
        def _():
            halo_copy(layer, True).wait_recv()

        @pl.when(row_rank < sp_size - 1)
        def _():
            halo_copy(layer, False).wait_recv()

    def halo_sent(layer):
        @pl.when(row_rank < sp_size - 1)
        def _():
            halo_copy(layer, True).wait_send()

        @pl.when(row_rank > 0)
        def _():
            halo_copy(layer, False).wait_send()

    groups = chans // GROUP

    def mix_matrix(layer):
        for g in range(groups):
            block = mix[layer, rank * groups + g].astype(jnp.float32)
            parts = [block if g == c else jnp.zeros((GROUP, GROUP), jnp.float32) for c in range(groups)]
            wide = parts[0] if groups == 1 else jnp.concatenate(parts, axis=1)
            bd[layer, g * GROUP : (g + 1) * GROUP, :] = wide.astype(jnp.bfloat16)

    def pool_chunk(layer, chunk):
        base = chunk * step_rows
        length = step_rows + 2 * HALO
        x = pad[layer, base : base + length, :]

        def ahead(v, n):
            return pltpu.roll(v, length - n, 0)

        sum1 = x + ahead(x, 1)
        sum2 = sum1 + ahead(sum1, 2)
        sum4 = sum2 + ahead(sum2, 4)
        sum8 = sum4 + ahead(sum4, 8)
        lane = lax.broadcasted_iota(jnp.int32, (step_rows, chans), 1)
        code = lax.rem(rank * groups + lane // GROUP, 4)
        position = row_rank * rows + base + lax.broadcasted_iota(jnp.int32, (step_rows, chans), 0)
        running = jnp.where(
            code == 0, ahead(sum1, 7)[:step_rows],
            jnp.where(
                code == 1, ahead(sum2, 6)[:step_rows],
                jnp.where(code == 2, ahead(sum4, 4)[:step_rows], sum8[:step_rows]),
            ),
        )
        window = jnp.where(code == 0, 1, jnp.where(code == 1, 2, jnp.where(code == 2, 4, 8)))
        counted = (jnp.minimum(position + window, total_rows) - jnp.maximum(position - window, 0)).astype(jnp.float32)
        pooled = (running / counted - x[HALO : HALO + step_rows]).astype(jnp.bfloat16)
        mixed = jnp.dot(pooled, bd[layer], preferred_element_type=jnp.float32)
        gate = acc_g[base : base + step_rows, :].astype(jnp.bfloat16).astype(jnp.float32)
        branch = mixed * (gate / (1.0 + jnp.exp(-gate)))
        br[layer, rank, pl.ds(base, step_rows), :] = branch.astype(jnp.bfloat16)

    def out_chunk(layer, chunk):
        span = pl.ds(chunk * step_rows, step_rows)
        total = hg[layer, rank, span, :].astype(jnp.float32)
        for k in range(tp_size):
            total = total + jnp.dot(
                br[layer, k, span, :], wo[layer, k * chans : (k + 1) * chans, :],
                preferred_element_type=jnp.float32,
            )
        if layer + 1 < layers:
            hg[layer + 1, rank, span, :] = total.astype(jnp.bfloat16)
        else:
            out[span, :] = total.astype(jnp.bfloat16)

    z_own(0)
    own_h.wait()
    for chunk in range(chunks):
        g_send(0, 0, chunk)
    for q in range(1, AHEAD):
        z_own(q)
    for layer in range(layers):
        mix_matrix(layer)
        for row in (0, rows + HALO):
            @pl.when(row_rank == (0 if row == 0 else sp_size - 1))
            def _():
                pad[layer, row : row + HALO, :] = jnp.zeros((HALO, chans), jnp.float32)

    per_layer = extra // layers * (sp_size - 1)

    def pace(layer, part):
        advance(layer * per_layer + int(per_layer * part + 0.1))

    for layer in range(layers):
        last = layer + 1 == layers
        for chunk in range(chunks):
            g_relay(0, layer, chunk)
            pace(layer, START[layer > 0] + (GATHERED[layer > 0] - START[layer > 0]) * (chunk + 1) / chunks)
            if chunk:
                g_arrived(0, layer, chunk - 1)
                normalize(layer, chunk - 1)
        g_arrived(0, layer, chunks - 1)
        normalize(layer, chunks - 1)
        y_arrived(layer, 0)
        project(acc_p, wi, layer)
        pad[layer, HALO : HALO + rows, :] = acc_p[...].astype(jnp.bfloat16).astype(jnp.float32)
        halo_send(layer)
        pace(layer, PROJECTED[layer > 0])
        y_arrived(layer, 1)
        project(acc_g, wg, layer)
        pace(layer, GATED[layer > 0])
        halo_arrived(layer)
        for chunk in range(chunks):
            pool_chunk(layer, chunk)
            g_send(1, layer, chunk)
        pace(layer, POOLED[layer > 0])
        for chunk in range(chunks):
            g_relay(1, layer, chunk)
        pace(layer, RELAYED[layer > 0])
        y_arrived(layer, 2)
        for chunk in range(chunks):
            g_arrived(1, layer, chunk)
            out_chunk(layer, chunk)
            if not last:
                g_send(0, layer + 1, chunk)
                pace(layer + 1, START[1] * chunk / chunks)
        if not last:
            pace(layer + 1, START[1])

    weights_sent()
    for layer in range(layers):
        halo_sent(layer)
        for kind in range(2):
            for chunk in range(chunks):
                g_sent(kind, layer, chunk)


def solution(mesh):
    sp_size, tp_size = mesh.shape["sp"], mesh.shape["tp"]

    def local(hidden_in, norm_gain, w_pool_in, w_pool_gate, group_mix, w_out):
        rows, cols = hidden_in.shape
        layers, _, chans = w_pool_in.shape
        width, channels = cols * tp_size, chans * tp_size
        chunks = rows // 128 if tp_size <= 4 else 1
        dims = (sp_size, tp_size, layers, rows, cols, chans, chunks)
        bf16, f32 = jnp.bfloat16, jnp.float32
        dma = pltpu.SemaphoreType.DMA
        hbm, vmem = pl.BlockSpec(memory_space=pl.ANY), pl.BlockSpec(memory_space=pltpu.VMEM)
        return pl.pallas_call(
            functools.partial(mixer, dims),
            out_shape=jax.ShapeDtypeStruct((rows, cols), bf16),
            in_specs=[hbm, vmem, hbm, hbm, vmem, hbm],
            out_specs=vmem,
            scratch_shapes=[
                pltpu.VMEM((layers, tp_size, rows, cols), bf16),
                pltpu.VMEM((tp_size, rows, cols), bf16),
                pltpu.VMEM((layers, tp_size, rows, chans), bf16),
                pltpu.VMEM((layers, width, chans), bf16),
                pltpu.VMEM((layers, width, chans), bf16),
                pltpu.VMEM((layers, channels, cols), bf16),
                pltpu.VMEM((layers, rows + 2 * HALO, chans), f32),
                pltpu.VMEM((rows, chans), f32),
                pltpu.VMEM((rows, chans), f32),
                pltpu.VMEM((layers, chans, chans), bf16),
                dma((1 + 3 * layers,)),
                dma((3 * layers * SUBS + 1, sp_size)),
                dma((3 * layers * SUBS + 1, sp_size + 1)),
                dma((3 * layers * SUBS + 1, sp_size)),
                dma((3 * layers * SUBS + 1, sp_size)),
                dma((2 * layers * chunks, tp_size)),
                dma((2 * layers * chunks, tp_size)),
                dma((layers, 2)),
                dma((layers, 2)),
            ],
            compiler_params=pltpu.CompilerParams(
                collective_id=0, has_side_effects=True, vmem_limit_bytes=60 * 1024 * 1024
            ),
        )(hidden_in, norm_gain, w_pool_in, w_pool_gate, group_mix, w_out)

    in_specs = (
        P(("grp", "sp"), "tp"),
        P(),
        P(None, "sp", "tp"),
        P(None, "sp", "tp"),
        P(),
        P(None, "sp", "tp"),
    )
    out_specs = P(("grp", "sp"), "tp")
    return jax.shard_map(local, mesh=mesh, in_specs=in_specs, out_specs=out_specs, check_vma=False)
```

profile of v0, /device:TPU:0, one launch (start us, length us, event | category | flops | bytes accessed | tf_op | source)
XLA Modules:
  0.0 132.6 jit_solution(8173802370792818186)
XLA Ops:
  0.0 130.1 %shard_map.64 = bf16[640,1024]{1,0:T(8,128)(2,1)} custom-call(bf16[640,1024]{1,0:T(8,128)(2,1)} %h_in.1, f32[2,4096]{1,0:T(2,128)} %gain.1, bf16[2,1024,256]{2,1,0:T(8,128)(2,1)} %w_in.1, bf16[2,1024,256]{2,1,0:T(8,128)(2,1)} %w_gate.1, bf16[2,16,64,64]{3,2,1,0:T(8,128)(2,1)} %mix.1, bf16[2,256,1024]{2,1,0:T(8,128)(2,1)} %w_out.1), custom_call_target="tpu_custom_call" | custom-call | tf_op jit(solution)/shard_map/pallas_call | solution.py:400
  130.2 2.5 %copy.8 = bf16[640,1024]{1,0:T(8,128)(2,1)} copy(bf16[640,1024]{1,0:T(8,128)(2,1)} %shard_map.64) | data formatting | bytes 2621440
where the time goes:
time: 133 us
  Pallas kernels  130 us (98%)
  local copies, waits for them, and re-layouts  2.47 us (2%)
    pallas_call x1, Pallas kernels, local(): pl.pallas_call(functools.partial(mixer, dims), out_shape=jax.ShapeDtypeSt...  130 us

commit v1 on v0

v1 whole, which is shorter than its diff:
```python
import functools

import jax
import jax.numpy as jnp
from jax import lax
from jax.experimental import pallas as pl
from jax.experimental.pallas import tpu as pltpu
from jax.sharding import PartitionSpec as P

GROUP = 64
HALO = 8
FULL = {(0, 0): ("inner",), (0, 1): ("inner",)}
NEAR = (0, 1, 3)
OUT_AFTER = 2
AHEAD = 2
MESH = pl.DeviceIdType.MESH

norm_eps = 1e-06


def guard(body, *conditions):
    traced = None
    for condition in conditions:
        if isinstance(condition, bool):
            if not condition:
                return
        else:
            traced = condition if traced is None else traced & condition
    if traced is None:
        body()
    else:
        pl.when(traced)(body)


def mixer(dims, h_in, gain, w_in, w_gate, mix, w_out, out, hg, hh, nb, nh, br, bh, wi, wg, wo, pad, acc_p, acc_g,
          gate_h, bd, local_sem, zr, zs, yr, ys, gr, gs, er, es, hs, tr, ts, pr, ps):
    sp_size, tp_size, layers, rows, cols, chans, chunks = dims
    step_rows = rows // chunks
    chips = tp_size // 2
    half = lax.axis_index("grp")
    row_rank = lax.axis_index("sp")
    rank = lax.axis_index("tp")
    chip, core = rank // 2, lax.rem(rank, 2)
    sibling = chip * 2 + 1 - core
    other = 1 - half
    total_rows = rows * sp_size
    last_row = sp_size - 1
    shards = ((w_in, wi), (w_gate, wg), (w_out, wo))
    up = jnp.minimum(row_rank + 1, last_row)
    down = jnp.maximum(row_rank - 1, 0)
    lower = row_rank < sp_size // 2
    at_end = (row_rank == 0) | (row_rank == last_row)
    host = True if sp_size == 4 else (row_rank == 1) | (row_rank == last_row - 1)
    inward = jnp.where(lower, up, down)
    outward = jnp.where(lower, down, up)

    def chip_rank(distance):
        return lax.rem(chip + distance, chips) * 2 + core

    def near(j):
        return j in NEAR

    def first(j):
        return pl.multiple_of(jnp.where(lower, chunks - 1 - j, j) * step_rows, step_rows)

    def span(j):
        return pl.ds(first(j), step_rows)

    own_w = {}
    for layer in range(layers):
        for t, (shard, whole) in enumerate(shards):
            depth = shard.shape[1]
            copy = pltpu.make_async_copy(
                shard.at[layer],
                whole.at[layer, pl.ds(pl.multiple_of(row_rank * depth, depth), depth)],
                local_sem.at[1 + layer * 3 + t],
            )
            copy.start()
            own_w[layer, t] = copy
    own_h = pltpu.make_async_copy(h_in, hg.at[0, rank], local_sem.at[0])
    own_h.start()

    barrier = pltpu.get_barrier_semaphore()
    peers = [
        {"sp": lax.rem(row_rank + 1, sp_size)},
        {"sp": lax.rem(row_rank + sp_size - 1, sp_size)},
        {"grp": other},
        {"tp": sibling},
    ] + [{"tp": chip_rank(d)} for d in range(1, chips)]
    for peer in peers:
        pl.semaphore_signal(barrier, inc=1, device_id=peer, device_id_type=MESH)
    pl.semaphore_wait(barrier, len(peers))

    streams = []
    for layer in range(layers):
        for t in range(3):
            streams.append((layer, t, "main"))
            streams.extend((layer, t, kind) for kind in FULL.get((layer, t), ()))

    def edge(q):
        return streams[q][0] == 0 and streams[q][1] < 2

    def member(kind, source):
        if kind == "inner":
            return (source > 0) & (source < last_row)
        if kind == "ends":
            return (source == 0) | (source == last_row)
        return True

    def swapped(layer, t, source):
        result = True
        for kind in FULL.get((layer, t), ()):
            absent = member(kind, source)
            absent = not absent if isinstance(absent, bool) else jnp.logical_not(absent)
            result = absent if result is True else result & absent
        return result

    def limits(q):
        return (1, last_row - 1) if edge(q) else (0, last_row)

    def piece_ref(layer, t, source, part):
        shard, whole = shards[t]
        depth = shard.shape[1]
        size = depth // 2
        start = pl.multiple_of(source * depth + part * size, size)
        return whole.at[layer, pl.ds(start, size)]

    def z_copy(q, source, to, send):
        layer, t, kind = streams[q]
        ref = piece_ref(layer, t, source, half if kind == "main" else other)
        return pltpu.make_async_remote_copy(
            ref, ref, zs.at[q, send], zr.at[q, source], device_id={"sp": to}, device_id_type=MESH
        )

    def y_copy(layer, t, source, part):
        ref = piece_ref(layer, t, source, part)
        return pltpu.make_async_remote_copy(
            ref, ref, ys.at[layer * 3 + t, source], yr.at[layer * 3 + t, source],
            device_id={"grp": other}, device_id_type=MESH,
        )

    def g_copy(kind, layer, j, source, to, send):
        ref = (hg, br)[kind].at[layer, source, span(j)]
        index = (kind * layers + layer) * chunks + j
        return pltpu.make_async_remote_copy(
            ref, ref, gs.at[index, send], gr.at[index, source], device_id={"tp": to}, device_id_type=MESH
        )

    def e_copy(j, source, to):
        return pltpu.make_async_remote_copy(
            hg.at[0, source, span(j)], hh.at[source, span(j)], es.at[j, source], er.at[j, source],
            device_id={"sp": to}, device_id_type=MESH,
        )

    def x_copy(j, source, to, send):
        ref = hh.at[source, span(j)]
        return pltpu.make_async_remote_copy(
            ref, ref, hs.at[j, send], er.at[j, source], device_id={"tp": to}, device_id_type=MESH
        )

    def t_copy(j, to):
        return pltpu.make_async_remote_copy(
            bh.at[span(j)], br.at[0, rank, span(j)], ts.at[j], tr.at[j], device_id={"sp": to}, device_id_type=MESH
        )

    def g_send(kind, layer, j):
        for d in range(1, chips):
            g_copy(kind, layer, j, rank, chip_rank(d), d).start()
        g_copy(kind, layer, j, rank, sibling, 0).start()

    def g_relay(kind, layer, j):
        for d in range(1, chips):
            source = chip_rank(d)
            g_copy(kind, layer, j, source, sibling, chips + d - 1).wait_recv()
            g_copy(kind, layer, j, source, sibling, chips + d - 1).start()

    def g_arrived(kind, layer, j):
        for d in range(chips):
            source = lax.rem(chip + d, chips) * 2 + 1 - core
            g_copy(kind, layer, j, source, sibling, 0).wait_recv()

    def g_sent(kind, layer, j):
        for d in range(1, chips):
            g_copy(kind, layer, j, rank, chip_rank(d), d).wait_send()
            g_copy(kind, layer, j, chip_rank(d), sibling, chips + d - 1).wait_send()
        g_copy(kind, layer, j, rank, sibling, 0).wait_send()

    def scaled(source, at, target, to, layer):
        squares = jnp.zeros((step_rows, 1), jnp.float32)
        for k in range(tp_size):
            block = source[k, at, :].astype(jnp.float32)
            squares = squares + jnp.sum(block * block, axis=1, keepdims=True)
        scaling = lax.rsqrt(squares / (cols * tp_size) + norm_eps)
        for k in range(tp_size):
            block = source[k, at, :].astype(jnp.float32)
            own_gain = gain[layer : layer + 1, k * cols : (k + 1) * cols]
            target[k, to, :] = (block * scaling * own_gain).astype(jnp.bfloat16)

    def normalize(layer, j):
        scaled(hg.at[layer], span(j), nb, span(j), layer)

    def project(acc, whole, layer):
        acc[...] = jnp.zeros_like(acc)

        @pl.loop(0, tp_size)
        def _(k):
            weight = whole[layer, pl.ds(pl.multiple_of(k * cols, cols), cols), :]
            acc[...] += jnp.dot(nb[k], weight, preferred_element_type=jnp.float32)

    def project_hosted(whole):
        total = jnp.zeros((step_rows, chans), jnp.float32)
        for k in range(tp_size):
            total = total + jnp.dot(nh[k], whole[0, k * cols : (k + 1) * cols, :], preferred_element_type=jnp.float32)
        return total.astype(jnp.bfloat16).astype(jnp.float32)

    own_shift = jnp.where(row_rank == 1, rows, 0)
    host_shift = jnp.where(row_rank == 1, 0, rows)
    groups = chans // GROUP

    def aligned(start):
        return pl.multiple_of(start, HALO)

    def halo_copy(layer, upward, shifted):
        if upward:
            source, target = rows + (own_shift if shifted else 0), 0
        else:
            source = HALO
            target = rows + HALO + (jnp.where(row_rank == 2, rows, 0) if shifted else 0)
        side = 0 if upward else 1
        return pltpu.make_async_remote_copy(
            pad.at[layer, pl.ds(aligned(source), HALO)], pad.at[layer, pl.ds(aligned(target), HALO)],
            ps.at[layer, side], pr.at[layer, side],
            device_id={"sp": up if upward else down}, device_id_type=MESH,
        )

    def halo_bounds(layer):
        return (1, last_row - 1) if layer == 0 else (0, last_row)

    def halo_send(layer):
        low, high = halo_bounds(layer)
        guard(lambda: halo_copy(layer, True, layer == 0).start(), row_rank < high)
        guard(lambda: halo_copy(layer, False, layer == 0).start(), row_rank > low)

    def halo_arrived(layer):
        low, high = halo_bounds(layer)
        guard(lambda: halo_copy(layer, True, False).wait_recv(), row_rank > low)
        guard(lambda: halo_copy(layer, False, False).wait_recv(), row_rank < high)

    def halo_sent(layer):
        low, high = halo_bounds(layer)
        guard(lambda: halo_copy(layer, True, False).wait_send(), row_rank < high)
        guard(lambda: halo_copy(layer, False, False).wait_send(), row_rank > low)

    def mix_matrix(layer):
        for g in range(groups):
            block = mix[layer, rank * groups + g].astype(jnp.float32)
            parts = [block if g == c else jnp.zeros((GROUP, GROUP), jnp.float32) for c in range(groups)]
            wide = parts[0] if groups == 1 else jnp.concatenate(parts, axis=1)
            bd[layer, g * GROUP : (g + 1) * GROUP, :] = wide.astype(jnp.bfloat16)

    def zero_pad(layer, start):
        pad[layer, start : start + HALO, :] = jnp.zeros((HALO, chans), jnp.float32)

    def gated(layer, j, shift, start, gate_ref):
        length = step_rows + 2 * HALO
        x = pad[layer, pl.ds(aligned(first(j) + shift), length), :]

        def ahead(v, n):
            return pltpu.roll(v, length - n, 0)

        sum1 = x + ahead(x, 1)
        sum2 = sum1 + ahead(sum1, 2)
        sum4 = sum2 + ahead(sum2, 4)
        sum8 = sum4 + ahead(sum4, 8)
        lane = lax.broadcasted_iota(jnp.int32, (step_rows, chans), 1)
        code = lax.rem(rank * groups + lane // GROUP, 4)
        position = start + first(j) + lax.broadcasted_iota(jnp.int32, (step_rows, chans), 0)
        running = jnp.where(
            code == 0, ahead(sum1, 7)[:step_rows],
            jnp.where(
                code == 1, ahead(sum2, 6)[:step_rows],
                jnp.where(code == 2, ahead(sum4, 4)[:step_rows], sum8[:step_rows]),
            ),
        )
        window = jnp.where(code == 0, 1, jnp.where(code == 1, 2, jnp.where(code == 2, 4, 8)))
        counted = (jnp.minimum(position + window, total_rows) - jnp.maximum(position - window, 0)).astype(jnp.float32)
        pooled = (running / counted - x[HALO : HALO + step_rows]).astype(jnp.bfloat16)
        mixed = jnp.dot(pooled, bd[layer], preferred_element_type=jnp.float32)
        gate = gate_ref[span(j), :].astype(jnp.bfloat16).astype(jnp.float32)
        return (mixed * (gate / (1.0 + jnp.exp(-gate)))).astype(jnp.bfloat16)

    def pool_chunk(layer, j):
        shift = own_shift if layer == 0 else 0
        br[layer, rank, span(j), :] = gated(layer, j, shift, row_rank * rows, acc_g)

    def pool_hosted(j):
        start = jnp.where(lower, row_rank - 1, row_rank + 1) * rows
        bh[span(j), :] = gated(0, j, host_shift, start, gate_h)
        t_copy(j, outward).start()

    def out_chunk(layer, j):
        total = hg[layer, rank, span(j), :].astype(jnp.float32)
        for k in range(tp_size):
            total = total + jnp.dot(
                br[layer, k, span(j), :], wo[layer, k * chans : (k + 1) * chans, :],
                preferred_element_type=jnp.float32,
            )
        if layer + 1 < layers:
            hg[layer + 1, rank, span(j), :] = total.astype(jnp.bfloat16)
        else:
            out[span(j), :] = total.astype(jnp.bfloat16)

    def y_wait(layer, t):
        for source in range(sp_size):
            guard(
                lambda source=source: y_copy(layer, t, source, other).wait_recv(),
                row_rank != source, swapped(layer, t, source),
            )

    def y_sent(layer, t):
        for source in range(sp_size):
            guard(
                lambda source=source: y_copy(layer, t, source, half).wait_send(),
                row_rank != source, swapped(layer, t, source),
            )

    def last_stream(layer, t):
        return max(q for q, stream in enumerate(streams) if stream[:2] == (layer, t))

    class Weights:
        def __init__(self, end):
            self.end = end
            self.loaded = set()
            self.owned = set()
            reach = range(1, sp_size) if end else range(1, last_row)
            order = [q for q in range(len(streams)) if not (end and edge(q))]
            if end:
                self.steps = [(q, 1) for q in order] + [(q, d) for q in order for d in reach if d > 1]
            else:
                self.steps = [(q, d) for q in order for d in reach]
            self.all = list(self.steps)

        def load(self, q):
            key = streams[q][:2]
            if key not in self.loaded:
                self.loaded.add(key)
                own_w[key].wait()

        def own(self, q, toward_end=False):
            kind = streams[q][2]
            low, high = limits(q)
            self.load(q)
            included = member(kind, row_rank)
            if self.end:
                guard(lambda: z_copy(q, row_rank, up, row_rank).start(), included, row_rank == 0)
                guard(lambda: z_copy(q, row_rank, down, sp_size).start(), included, row_rank == last_row)
                return
            if not toward_end and q in self.owned:
                return
            if not toward_end:
                self.owned.add(q)
            up_end, down_end = row_rank == last_row - 1, row_rank == 1
            if not toward_end:
                up_end, down_end = jnp.logical_not(up_end), jnp.logical_not(down_end)
            guard(lambda: z_copy(q, row_rank, up, row_rank).start(), included, row_rank + 1 <= high, up_end)
            guard(lambda: z_copy(q, row_rank, down, sp_size).start(), included, row_rank - 1 >= low, down_end)

        def step(self, q, distance):
            layer, t, kind = streams[q]
            bottom, top = limits(q)
            low, high = row_rank - distance, row_rank + distance

            def take(source, onward, to):
                copy = z_copy(q, source, to, source)
                copy.wait_recv()
                if not self.end:
                    guard(lambda: z_copy(q, source, to, source).start(), onward)
                if kind == "main":
                    guard(lambda: y_copy(layer, t, source, half).start(), swapped(layer, t, source))

            guard(lambda: take(low, row_rank + 1 <= top, up), low >= 0, member(kind, low))
            guard(lambda: take(high, row_rank - 1 >= bottom, down), high <= last_row, member(kind, high))

        def advance(self, count):
            while self.steps and len(self.all) - len(self.steps) < count:
                q, d = self.steps.pop(0)
                self.step(q, d)
                if not self.end and d == last_row - 1:
                    for later in range(q + 1, min(q + 1 + AHEAD, len(streams))):
                        self.own(later)

        def upto(self, layer, t, distance=None):
            q = last_stream(layer, t)
            reach = [d for p, d in self.all if p == q]
            self.advance(self.all.index((q, reach[-1] if distance is None else distance)) + 1)

        def arrived(self, layer, t):
            self.upto(layer, t)
            y_wait(layer, t)

        def finish(self):
            self.advance(len(self.all))
            for q, (layer, t, kind) in enumerate(streams):
                low, high = limits(q)
                if self.end:
                    included = member(kind, row_rank)
                    guard(lambda: z_copy(q, row_rank, up, row_rank).wait_send(), included, row_rank == 0)
                    guard(lambda: z_copy(q, row_rank, down, sp_size).wait_send(), included, row_rank == last_row)
                else:
                    for source in range(sp_size):
                        included = member(kind, source)
                        copy = z_copy(q, source, up, source)
                        guard(lambda: copy.wait_send(), included, source <= row_rank, row_rank + 1 <= high)
                        guard(lambda: copy.wait_send(), included, source > row_rank, row_rank - 1 >= low)
                    guard(
                        lambda: z_copy(q, row_rank, down, sp_size).wait_send(),
                        member(kind, row_rank), row_rank - 1 >= low,
                    )
                if kind == "main" and not (self.end and edge(q)):
                    y_sent(layer, t)

    def host_take(j):
        e_copy(j, rank, outward).wait_recv()
        if not near(j):
            for d in range(1, chips):
                x_copy(j, rank, chip_rank(d), d).start()
        x_copy(j, rank, sibling, chips).start()

    def host_relay(j):
        for d in range(1, chips):
            source = chip_rank(d)
            e_copy(j, source, outward).wait_recv()
            x_copy(j, source, sibling, chips + d).start()

    def host_arrived(j):
        for d in range(chips):
            source = lax.rem(chip + d, chips) * 2 + 1 - core
            e_copy(j, source, outward).wait_recv()

    def host_sent(j):
        if not near(j):
            for d in range(1, chips):
                x_copy(j, rank, chip_rank(d), d).wait_send()
        for d in range(chips):
            x_copy(j, chip_rank(d), sibling, chips + d).wait_send()
        t_copy(j, outward).wait_send()

    def host_project(j):
        scaled(hh, span(j), nh, pl.ds(0, step_rows), 0)
        pad[0, pl.ds(aligned(HALO + host_shift + first(j)), step_rows), :] = project_hosted(wi)
        gate_h[span(j), :] = project_hosted(wg)

    def own_project(weights, layer, shift):
        weights.arrived(layer, 0)
        project(acc_p, wi, layer)
        pad[layer, pl.ds(aligned(HALO + shift), rows), :] = acc_p[...].astype(jnp.bfloat16).astype(jnp.float32)
        halo_send(layer)

    def later_layers(weights, ready):
        for layer in range(1, layers):
            last = layer + 1 == layers
            for j in range(chunks):
                if layer == 1 and j < ready:
                    continue
                g_relay(0, layer, j)
                g_arrived(0, layer, j)
                normalize(layer, j)
            own_project(weights, layer, 0)
            weights.upto(layer, 1)
            weights.arrived(layer, 1)
            project(acc_g, wg, layer)
            weights.upto(layer, 2, 1)
            halo_arrived(layer)
            for j in range(chunks):
                pool_chunk(layer, j)
                g_send(1, layer, j)
            for j in range(chunks):
                g_relay(1, layer, j)
            weights.arrived(layer, 2)
            for j in range(chunks):
                g_arrived(1, layer, j)
                out_chunk(layer, j)
                if not last:
                    g_send(0, layer + 1, j)

    def all_sent(weights):
        weights.finish()
        for layer in range(1, layers):
            halo_sent(layer)
            for j in range(chunks):
                g_sent(0, layer, j)
                g_sent(1, layer, j)

    def end_program():
        weights = Weights(True)
        order = range(len(streams))
        for q in order:
            if edge(q):
                weights.own(q)
        own_h.wait()
        for j in range(chunks):
            if near(j):
                for d in range(1, chips):
                    g_copy(0, 0, j, rank, chip_rank(d), d).start()
        for j in range(chunks):
            e_copy(j, rank, inward).start()
            if near(j):
                for d in range(1, chips):
                    source = chip_rank(d)
                    g_copy(0, 0, j, source, sibling, 0).wait_recv()
                    e_copy(j, source, inward).start()
            if j == min(1, chunks - 1):
                for q in order:
                    if streams[q][:2] == (0, 2):
                        weights.own(q)
        for q in order:
            if not edge(q) and streams[q][:2] != (0, 2):
                weights.own(q)
        for layer in range(layers):
            mix_matrix(layer)
            if layer:
                guard(lambda: zero_pad(layer, 0), row_rank == 0)
                guard(lambda: zero_pad(layer, rows + HALO), row_rank == last_row)
        weights.advance(sum(1 for _, d in weights.all if d == 1))
        weights.arrived(0, 2)
        for j in range(chunks):
            t_copy(j, inward).wait_recv()
            g_send(1, 0, j)
            g_relay(1, 0, j)
            if j:
                g_relay(0, 1, j - 1)
            g_arrived(1, 0, j)
            out_chunk(0, j)
            g_send(0, 1, j)
            if j:
                g_arrived(0, 1, j - 1)
                normalize(1, j - 1)
        later_layers(weights, chunks - 1)
        all_sent(weights)
        for j in range(chunks):
            g_sent(1, 0, j)
            e_copy(j, rank, inward).wait_send()
            if near(j):
                for d in range(1, chips):
                    g_copy(0, 0, j, rank, chip_rank(d), d).wait_send()
                    e_copy(j, chip_rank(d), inward).wait_send()

    def mid_program():
        weights = Weights(False)
        own_h.wait()
        for q in range(1 + AHEAD):
            weights.own(q)
        for j in range(chunks):
            g_send(0, 0, j)
        for q in range(len(streams)):
            if not edge(q):
                weights.own(q, True)
        for layer in range(layers):
            mix_matrix(layer)
        guard(lambda: zero_pad(0, 0), row_rank == 1)
        guard(lambda: zero_pad(0, 2 * rows + HALO), row_rank == last_row - 1)
        entry = len([1 for q, _ in weights.all if edge(q)])
        for j in range(chunks):
            g_relay(0, 0, j)
            weights.advance(entry * (j + 1) // (chunks + 1))
            if j:
                g_arrived(0, 0, j - 1)
                normalize(0, j - 1)
        g_arrived(0, 0, chunks - 1)
        normalize(0, chunks - 1)
        guard(lambda: host_take(0), host)
        guard(lambda: host_relay(0), host)
        own_project(weights, 0, own_shift)
        weights.arrived(0, 1)
        project(acc_g, wg, 0)

        def own_pool():
            halo_arrived(0)
            for j in range(chunks):
                pool_chunk(0, j)
                g_send(1, 0, j)

        def own_out():
            for j in range(chunks):
                g_relay(1, 0, j)
            weights.arrived(0, 2)
            for j in range(chunks):
                g_arrived(1, 0, j)
                out_chunk(0, j)
                g_send(0, 1, j)

        tail = [q for q, d in weights.all if not edge(q)]
        for j in range(chunks):
            if j:
                guard(lambda: host_take(j), host)
                guard(lambda: host_relay(j), host)
            guard(lambda: host_arrived(j), host)
            guard(lambda: host_project(j), host)
            if j:
                guard(lambda: pool_hosted(j - 1), host)
            else:
                own_pool()
            if j == min(OUT_AFTER, chunks - 1):
                own_out()
            if j > OUT_AFTER:
                weights.upto(1, 0, 1 if j == OUT_AFTER + 1 else None)
        guard(lambda: pool_hosted(chunks - 1), host)
        later_layers(weights, 0)
        all_sent(weights)
        halo_sent(0)
        for j in range(chunks):
            g_sent(0, 0, j)
            g_sent(1, 0, j)
            guard(lambda: host_sent(j), host)

    pl.when(at_end)(end_program)
    pl.when(jnp.logical_not(at_end))(mid_program)


def solution(mesh):
    sp_size, tp_size = mesh.shape["sp"], mesh.shape["tp"]

    def local(hidden_in, norm_gain, w_pool_in, w_pool_gate, group_mix, w_out):
        rows, cols = hidden_in.shape
        layers, _, chans = w_pool_in.shape
        width, channels = cols * tp_size, chans * tp_size
        chunks = rows // 128 if tp_size <= 4 else 1
        streams = 3 * layers + sum(len(kinds) for kinds in FULL.values())
        dims = (sp_size, tp_size, layers, rows, cols, chans, chunks)
        bf16, f32 = jnp.bfloat16, jnp.float32
        dma = pltpu.SemaphoreType.DMA
        hbm, vmem = pl.BlockSpec(memory_space=pl.ANY), pl.BlockSpec(memory_space=pltpu.VMEM)
        return pl.pallas_call(
            functools.partial(mixer, dims),
            out_shape=jax.ShapeDtypeStruct((rows, cols), bf16),
            in_specs=[hbm, vmem, hbm, hbm, vmem, hbm],
            out_specs=vmem,
            scratch_shapes=[
                pltpu.VMEM((layers, tp_size, rows, cols), bf16),
                pltpu.VMEM((tp_size, rows, cols), bf16),
                pltpu.VMEM((tp_size, rows, cols), bf16),
                pltpu.VMEM((tp_size, rows // chunks, cols), bf16),
                pltpu.VMEM((layers, tp_size, rows, chans), bf16),
                pltpu.VMEM((rows, chans), bf16),
                pltpu.VMEM((layers, width, chans), bf16),
                pltpu.VMEM((layers, width, chans), bf16),
                pltpu.VMEM((layers, channels, cols), bf16),
                pltpu.VMEM((layers, 2 * rows + 2 * HALO, chans), f32),
                pltpu.VMEM((rows, chans), f32),
                pltpu.VMEM((rows, chans), f32),
                pltpu.VMEM((rows, chans), f32),
                pltpu.VMEM((layers, chans, chans), bf16),
                dma((1 + 3 * layers,)),
                dma((streams, sp_size)),
                dma((streams, sp_size + 1)),
                dma((3 * layers, sp_size)),
                dma((3 * layers, sp_size)),
                dma((2 * layers * chunks, tp_size)),
                dma((2 * layers * chunks, tp_size)),
                dma((chunks, tp_size)),
                dma((chunks, tp_size)),
                dma((chunks, tp_size)),
                dma((chunks,)),
                dma((chunks,)),
                dma((layers, 2)),
                dma((layers, 2)),
            ],
            compiler_params=pltpu.CompilerParams(
                collective_id=0, has_side_effects=True, vmem_limit_bytes=60 * 1024 * 1024
            ),
        )(hidden_in, norm_gain, w_pool_in, w_pool_gate, group_mix, w_out)

    in_specs = (
        P(("grp", "sp"), "tp"),
        P(),
        P(None, "sp", "tp"),
        P(None, "sp", "tp"),
        P(),
        P(None, "sp", "tp"),
    )
    out_specs = P(("grp", "sp"), "tp")
    return jax.shard_map(local, mesh=mesh, in_specs=in_specs, out_specs=out_specs, check_vma=False)
```

time: 133 us -> 213 us (1.60)
  Pallas kernels: 130 us -> 210 us
    pallas_call x1, Pallas kernels: 130 us -> 210 us  [local(): pl.pallas_call(functools.partial(mixer, dims), out_shape=jax.ShapeDtypeSt...]
where the time goes in v1:
time: 213 us
  Pallas kernels  210 us (99%)
  local copies, waits for them, and re-layouts  2.47 us (1%)
    pallas_call x1, Pallas kernels, local(): pl.pallas_call(functools.partial(mixer, dims), out_shape=jax.ShapeDtypeSt...  210 us

profile of v1, /device:TPU:0, one launch (start us, length us, event | category | flops | bytes accessed | tf_op | source)
XLA Modules:
  0.0 212.7 jit_solution(1949270830691717006)
XLA Ops:
  0.0 210.2 %shard_map.64 = bf16[640,1024]{1,0:T(8,128)(2,1)} custom-call(bf16[640,1024]{1,0:T(8,128)(2,1)} %h_in.1, f32[2,4096]{1,0:T(2,128)} %gain.1, bf16[2,1024,256]{2,1,0:T(8,128)(2,1)} %w_in.1, bf16[2,1024,256]{2,1,0:T(8,128)(2,1)} %w_gate.1, bf16[2,16,64,64]{3,2,1,0:T(8,128)(2,1)} %mix.1, bf16[2,256,1024]{2,1,0:T(8,128)(2,1)} %w_out.1), custom_call_target="tpu_custom_call" | custom-call | tf_op jit(solution)/shard_map/pallas_call | solution.py:633
  210.2 2.5 %copy.8 = bf16[640,1024]{1,0:T(8,128)(2,1)} copy(bf16[640,1024]{1,0:T(8,128)(2,1)} %shard_map.64) | data formatting | bytes 2621440

commit v2 on v1

--- a/solution.py
+++ b/solution.py
@@ -9,10 +9,12 @@
 
 GROUP = 64
 HALO = 8
-FULL = {(0, 0): ("inner",), (0, 1): ("inner",)}
-NEAR = (0, 1, 3)
-OUT_AFTER = 2
-AHEAD = 2
+FULL = {(0, 0): ("core",), (1, 0): ("near",), (1, 1): ("near",), (1, 2): ("near",)}
+NEAR = (4,)
+SEND = ('k', 'cs', 'k', 'k', 'k', 'ds', 'k', 'es', 'fs', 'ps', 'qs', 'rs')
+EARLY = "cdef"
+MID = ('ao', 'ai1', 'r', 'bo', 'bi1', 'xs', 'cs', 'r', 'n', 'ai', 'k', 'r', 'n', 'bi', 'co', 'r', 'n', 'k', 'xi', 'r', 'n', 'ci1', 'k', 'n', 'p', 'ds', 'g', 'ci', 'es', 'k', 'h', 'h', 'di1', 'o', 'h', 'do', 'h', 'fs', 'k', 'ei1', 'h', 'R', 'O', 'di', 'eo', 'fo', 'q', 'm', 'ei', 'fi1', 'q', 'm', 'fi', 'po', 'A', 'i', 'i', 'q', 'm', 'qo', 'i', 'E', 'e', 'e', 'e', 'q', 'm', 'i', 'e', 'b', 'b', 'b', 'ro', 'q', 'm', 'i', 'e', 'b', 'b', 'x', 'x', 'x', 'x', 'x', 'F', 'z', 'z', 'z', 'z', 'z')
+END = ('ci1', 'di1', 'ei1', 'fi1', 'ci2', 'ci', 't', 't', 'Y', 'o', 'di2', 't', 'o', 't', 't', 'o', 'ei2', 'o', 'di', 'o', 'q', 'm', 'q', 'm', 'ei', 'q', 'm', 'A', 'i', 'i', 'i', 'fi2', 'q', 'm', 'i', 'E', 'e', 'e', 'b', 'e', 'b', 'fi', 'e', 'b', 'q', 'm', 'i', 'e', 'b', 'x', 'x', 'b', 'x', 'x', 'x', 'F', 'z', 'z', 'z', 'z', 'z')
 MESH = pl.DeviceIdType.MESH
 
 norm_eps = 1e-06
@@ -33,7 +35,7 @@
 
 
 def mixer(dims, h_in, gain, w_in, w_gate, mix, w_out, out, hg, hh, nb, nh, br, bh, wi, wg, wo, pad, acc_p, acc_g,
-          gate_h, bd, local_sem, zr, zs, yr, ys, gr, gs, er, es, hs, tr, ts, pr, ps):
+          gate_h, bd, local_sem, out_sem, zr, zs, yr, ys, gr, gs, er, es, hs, tr, ts, pr, ps):
     sp_size, tp_size, layers, rows, cols, chans, chunks = dims
     step_rows = rows // chunks
     chips = tp_size // 2
@@ -91,26 +93,28 @@
         pl.semaphore_signal(barrier, inc=1, device_id=peer, device_id_type=MESH)
     pl.semaphore_wait(barrier, len(peers))
 
-    streams = []
-    for layer in range(layers):
-        for t in range(3):
-            streams.append((layer, t, "main"))
-            streams.extend((layer, t, kind) for kind in FULL.get((layer, t), ()))
+    streams = [(layer, t, "main") for layer in range(layers) for t in range(3)]
+    streams += [(layer, t, kind) for (layer, t), kinds in FULL.items() for kind in kinds]
 
     def edge(q):
-        return streams[q][0] == 0 and streams[q][1] < 2
+        layer, t, kind = streams[q]
+        return kind in ("core", "near") or (layer == 0 and t < 2)
 
     def member(kind, source):
-        if kind == "inner":
+        if kind in ("inner", "core"):
             return (source > 0) & (source < last_row)
-        if kind == "ends":
+        if kind == "near":
             return (source == 0) | (source == last_row)
         return True
 
-    def swapped(layer, t, source):
+    def swapped(layer, t, source, end):
         result = True
         for kind in FULL.get((layer, t), ()):
+            if end and kind == "core":
+                continue
             absent = member(kind, source)
+            if kind == "near":
+                absent = ((source == 0) & (row_rank == 1)) | ((source == last_row) & (row_rank == last_row - 1))
             absent = not absent if isinstance(absent, bool) else jnp.logical_not(absent)
             result = absent if result is True else result & absent
         return result
@@ -143,24 +147,27 @@
         ref = (hg, br)[kind].at[layer, source, span(j)]
         index = (kind * layers + layer) * chunks + j
         return pltpu.make_async_remote_copy(
-            ref, ref, gs.at[index, send], gr.at[index, source], device_id={"tp": to}, device_id_type=MESH
+            ref, ref, gs.at[kind * layers + layer, send], gr.at[index, source], device_id={"tp": to}, device_id_type=MESH
         )
 
     def e_copy(j, source, to):
         return pltpu.make_async_remote_copy(
-            hg.at[0, source, span(j)], hh.at[source, span(j)], es.at[j, source], er.at[j, source],
+            hg.at[0, source, span(j)], hh.at[source, span(j)], es.at[source], er.at[j, source],
             device_id={"sp": to}, device_id_type=MESH,
         )
 
     def x_copy(j, source, to, send):
         ref = hh.at[source, span(j)]
         return pltpu.make_async_remote_copy(
-            ref, ref, hs.at[j, send], er.at[j, source], device_id={"tp": to}, device_id_type=MESH
+            ref, ref, hs.at[send], er.at[j, source], device_id={"tp": to}, device_id_type=MESH
         )
+
+    def o_copy(j):
+        return pltpu.make_async_copy(nb.at[0, span(j)], out.at[span(j)], out_sem.at[j])
 
     def t_copy(j, to):
         return pltpu.make_async_remote_copy(
-            bh.at[span(j)], br.at[0, rank, span(j)], ts.at[j], tr.at[j], device_id={"sp": to}, device_id_type=MESH
+            bh.at[span(j)], br.at[0, rank, span(j)], ts.at[0], tr.at[j], device_id={"sp": to}, device_id_type=MESH
         )
 
     def g_send(kind, layer, j):
@@ -179,11 +186,17 @@
             source = lax.rem(chip + d, chips) * 2 + 1 - core
             g_copy(kind, layer, j, source, sibling, 0).wait_recv()
 
-    def g_sent(kind, layer, j):
-        for d in range(1, chips):
-            g_copy(kind, layer, j, rank, chip_rank(d), d).wait_send()
-            g_copy(kind, layer, j, chip_rank(d), sibling, chips + d - 1).wait_send()
-        g_copy(kind, layer, j, rank, sibling, 0).wait_send()
+    def flushed(ref, sem, count=chunks):
+        if count:
+            part = ref.at[pl.ds(0, count * step_rows)]
+            pltpu.make_async_remote_copy(
+                part, part, sem, gr.at[0, 0], device_id={"tp": sibling}, device_id_type=MESH
+            ).wait_send()
+
+    def g_sent(kind, layer):
+        ref = (hg, br)[kind].at[layer, rank]
+        for slot in range(2 * chips - 1):
+            flushed(ref, gs.at[kind * layers + layer, slot])
 
     def scaled(source, at, target, to, layer):
         squares = jnp.zeros((step_rows, 1), jnp.float32)
@@ -241,10 +254,21 @@
         guard(lambda: halo_copy(layer, True, layer == 0).start(), row_rank < high)
         guard(lambda: halo_copy(layer, False, layer == 0).start(), row_rank > low)
 
+    def halo_side(layer, inner):
+        low, high = halo_bounds(layer)
+        rising = lower if inner else jnp.logical_not(lower)
+        guard(lambda: halo_copy(layer, True, layer == 0).start(), rising, row_rank < high)
+        guard(lambda: halo_copy(layer, False, layer == 0).start(), jnp.logical_not(rising), row_rank > low)
+
     def halo_arrived(layer):
         low, high = halo_bounds(layer)
         guard(lambda: halo_copy(layer, True, False).wait_recv(), row_rank > low)
         guard(lambda: halo_copy(layer, False, False).wait_recv(), row_rank < high)
+
+    def halo_wait(layer, inner):
+        rising = jnp.logical_not(lower) if inner else lower
+        guard(lambda: halo_copy(layer, True, False).wait_recv(), rising, row_rank > 0)
+        guard(lambda: halo_copy(layer, False, False).wait_recv(), jnp.logical_not(rising), row_rank < last_row)
 
     def halo_sent(layer):
         low, high = halo_bounds(layer)
@@ -308,37 +332,31 @@
         if layer + 1 < layers:
             hg[layer + 1, rank, span(j), :] = total.astype(jnp.bfloat16)
         else:
-            out[span(j), :] = total.astype(jnp.bfloat16)
-
-    def y_wait(layer, t):
+            nb[0, span(j), :] = total.astype(jnp.bfloat16)
+
+    def y_wait(layer, t, end):
         for source in range(sp_size):
             guard(
                 lambda source=source: y_copy(layer, t, source, other).wait_recv(),
-                row_rank != source, swapped(layer, t, source),
+                row_rank != source, swapped(layer, t, source, end),
             )
 
-    def y_sent(layer, t):
+    def y_sent(layer, t, end):
         for source in range(sp_size):
             guard(
                 lambda source=source: y_copy(layer, t, source, half).wait_send(),
-                row_rank != source, swapped(layer, t, source),
+                row_rank != source, swapped(layer, t, source, end),
             )
 
-    def last_stream(layer, t):
-        return max(q for q, stream in enumerate(streams) if stream[:2] == (layer, t))
+    names = {letter: (i // 3, i % 3, "main") for i, letter in enumerate("abcdef")}
+    names.update(p=(1, 0, "near"), q=(1, 1, "near"), r=(1, 2, "near"), x=(0, 0, "core"), y=(0, 1, "core"), w=(0, 2, "inner"), v=(1, 0, "core"), u=(1, 1, "core"))
 
     class Weights:
         def __init__(self, end):
             self.end = end
             self.loaded = set()
             self.owned = set()
-            reach = range(1, sp_size) if end else range(1, last_row)
-            order = [q for q in range(len(streams)) if not (end and edge(q))]
-            if end:
-                self.steps = [(q, 1) for q in order] + [(q, d) for q in order for d in reach if d > 1]
-            else:
-                self.steps = [(q, d) for q in order for d in reach]
-            self.all = list(self.steps)
+            self.done = set()
 
         def load(self, q):
             key = streams[q][:2]
@@ -351,73 +369,97 @@
             low, high = limits(q)
             self.load(q)
             included = member(kind, row_rank)
+            if not toward_end:
+                if q in self.owned:
+                    return
+                self.owned.add(q)
             if self.end:
                 guard(lambda: z_copy(q, row_rank, up, row_rank).start(), included, row_rank == 0)
                 guard(lambda: z_copy(q, row_rank, down, sp_size).start(), included, row_rank == last_row)
                 return
-            if not toward_end and q in self.owned:
-                return
-            if not toward_end:
-                self.owned.add(q)
             up_end, down_end = row_rank == last_row - 1, row_rank == 1
             if not toward_end:
                 up_end, down_end = jnp.logical_not(up_end), jnp.logical_not(down_end)
             guard(lambda: z_copy(q, row_rank, up, row_rank).start(), included, row_rank + 1 <= high, up_end)
             guard(lambda: z_copy(q, row_rank, down, sp_size).start(), included, row_rank - 1 >= low, down_end)
 
-        def step(self, q, distance):
+        def step(self, q, outer, distance):
+            if (q, outer, distance) in self.done or (self.end and edge(q)):
+                return
+            self.done.add((q, outer, distance))
             layer, t, kind = streams[q]
             bottom, top = limits(q)
-            low, high = row_rank - distance, row_rank + distance
-
-            def take(source, onward, to):
-                copy = z_copy(q, source, to, source)
-                copy.wait_recv()
+            below = lower if outer else jnp.logical_not(lower)
+            source = jnp.where(below, row_rank - distance, row_rank + distance)
+            onward = jnp.where(below, row_rank + 1 <= top, row_rank - 1 >= bottom)
+            if kind == "near":
+                if not outer or distance > 1:
+                    return
+                onward = False
+            to = jnp.where(below, up, down)
+
+            def take():
+                z_copy(q, source, to, source).wait_recv()
                 if not self.end:
                     guard(lambda: z_copy(q, source, to, source).start(), onward)
                 if kind == "main":
-                    guard(lambda: y_copy(layer, t, source, half).start(), swapped(layer, t, source))
-
-            guard(lambda: take(low, row_rank + 1 <= top, up), low >= 0, member(kind, low))
-            guard(lambda: take(high, row_rank - 1 >= bottom, down), high <= last_row, member(kind, high))
-
-        def advance(self, count):
-            while self.steps and len(self.all) - len(self.steps) < count:
-                q, d = self.steps.pop(0)
-                self.step(q, d)
-                if not self.end and d == last_row - 1:
-                    for later in range(q + 1, min(q + 1 + AHEAD, len(streams))):
-                        self.own(later)
-
-        def upto(self, layer, t, distance=None):
-            q = last_stream(layer, t)
-            reach = [d for p, d in self.all if p == q]
-            self.advance(self.all.index((q, reach[-1] if distance is None else distance)) + 1)
+                    guard(lambda: y_copy(layer, t, source, half).start(), swapped(layer, t, source, self.end))
+
+            guard(take, source >= 0, source <= last_row, member(kind, source))
+
+        def outer(self, q):
+            if not self.end:
+                for d in range(1, sp_size // 2):
+                    self.step(q, True, d)
+
+        def inner(self, q, reach=None):
+            for d in range(1, (sp_size if self.end else sp_size - 1) if reach is None else reach + 1):
+                self.step(q, False, d)
+
+        def word(self, word):
+            if names[word[0]] not in streams:
+                return
+            q = streams.index(names[word[0]])
+            if word[1] == "s":
+                self.own(q)
+            elif word[1] == "o":
+                self.outer(q)
+            else:
+                self.inner(q, int(word[2:]) if word[2:] else None)
+
+        def settle(self, layer, t):
+            for q, stream in enumerate(streams):
+                if stream[:2] == (layer, t):
+                    self.own(q)
+                    self.outer(q)
+                    self.inner(q)
 
         def arrived(self, layer, t):
-            self.upto(layer, t)
-            y_wait(layer, t)
+            self.settle(layer, t)
+            y_wait(layer, t, self.end)
 
         def finish(self):
-            self.advance(len(self.all))
             for q, (layer, t, kind) in enumerate(streams):
                 low, high = limits(q)
                 if self.end:
                     included = member(kind, row_rank)
                     guard(lambda: z_copy(q, row_rank, up, row_rank).wait_send(), included, row_rank == 0)
                     guard(lambda: z_copy(q, row_rank, down, sp_size).wait_send(), included, row_rank == last_row)
-                else:
+                elif kind != "near":
                     for source in range(sp_size):
                         included = member(kind, source)
-                        copy = z_copy(q, source, up, source)
-                        guard(lambda: copy.wait_send(), included, source <= row_rank, row_rank + 1 <= high)
-                        guard(lambda: copy.wait_send(), included, source > row_rank, row_rank - 1 >= low)
+
+                        def sent(source=source):
+                            z_copy(q, source, up, source).wait_send()
+
+                        guard(sent, included, source <= row_rank, row_rank + 1 <= high)
+                        guard(sent, included, source > row_rank, row_rank - 1 >= low)
                     guard(
                         lambda: z_copy(q, row_rank, down, sp_size).wait_send(),
                         member(kind, row_rank), row_rank - 1 >= low,
                     )
                 if kind == "main" and not (self.end and edge(q)):
-                    y_sent(layer, t)
+                    y_sent(layer, t, self.end)
 
     def host_take(j):
         e_copy(j, rank, outward).wait_recv()
@@ -437,18 +479,33 @@
             source = lax.rem(chip + d, chips) * 2 + 1 - core
             e_copy(j, source, outward).wait_recv()
 
-    def host_sent(j):
-        if not near(j):
-            for d in range(1, chips):
-                x_copy(j, rank, chip_rank(d), d).wait_send()
+    few = sum(1 for j in range(chunks) if near(j))
+
+    def host_sent():
+        for d in range(1, chips):
+            flushed(hh.at[rank], hs.at[d], chunks - few)
         for d in range(chips):
-            x_copy(j, chip_rank(d), sibling, chips + d).wait_send()
-        t_copy(j, outward).wait_send()
+            flushed(hh.at[rank], hs.at[chips + d])
+        flushed(bh, ts.at[0])
 
     def host_project(j):
         scaled(hh, span(j), nh, pl.ds(0, step_rows), 0)
         pad[0, pl.ds(aligned(HALO + host_shift + first(j)), step_rows), :] = project_hosted(wi)
         gate_h[span(j), :] = project_hosted(wg)
+
+    def project_chunk(whole, layer, j):
+        total = jnp.zeros((step_rows, chans), jnp.float32)
+        for k in range(tp_size):
+            weight = whole[layer, k * cols : (k + 1) * cols, :]
+            total = total + jnp.dot(nb[k, span(j), :], weight, preferred_element_type=jnp.float32)
+        return total
+
+    def in_chunk(layer, j):
+        rounded = project_chunk(wi, layer, j).astype(jnp.bfloat16).astype(jnp.float32)
+        pad[layer, pl.ds(aligned(HALO + first(j)), step_rows), :] = rounded
+
+    def gate_chunk(layer, j):
+        acc_g[span(j), :] = project_chunk(wg, layer, j)
 
     def own_project(weights, layer, shift):
         weights.arrived(layer, 0)
@@ -456,165 +513,201 @@
         pad[layer, pl.ds(aligned(HALO + shift), rows), :] = acc_p[...].astype(jnp.bfloat16).astype(jnp.float32)
         halo_send(layer)
 
-    def later_layers(weights, ready):
-        for layer in range(1, layers):
-            last = layer + 1 == layers
+    def emit_last(layer, j):
+        g_arrived(1, layer, j)
+        out_chunk(layer, j)
+        if layer + 1 == layers:
+            o_copy(j).start()
+        else:
+            g_send(0, layer + 1, j)
+
+    def later_layers(weights):
+        for layer in range(2, layers):
+            weights.arrived(layer, 0)
             for j in range(chunks):
-                if layer == 1 and j < ready:
-                    continue
                 g_relay(0, layer, j)
                 g_arrived(0, layer, j)
                 normalize(layer, j)
-            own_project(weights, layer, 0)
-            weights.upto(layer, 1)
+                in_chunk(layer, j)
+            halo_side(layer, True)
+            halo_side(layer, False)
             weights.arrived(layer, 1)
-            project(acc_g, wg, layer)
-            weights.upto(layer, 2, 1)
             halo_arrived(layer)
             for j in range(chunks):
+                gate_chunk(layer, j)
                 pool_chunk(layer, j)
                 g_send(1, layer, j)
             for j in range(chunks):
                 g_relay(1, layer, j)
             weights.arrived(layer, 2)
             for j in range(chunks):
-                g_arrived(1, layer, j)
-                out_chunk(layer, j)
-                if not last:
-                    g_send(0, layer + 1, j)
+                emit_last(layer, j)
+
+    def second_layer(weights, end):
+        def place(j):
+            return j if end else chunks - 1 - j
+
+        def ready(j):
+            in_chunk(1, place(j))
+            if place(j) == 0:
+                halo_side(1, True)
+            if place(j) == chunks - 1:
+                halo_side(1, False)
+
+        def branch(j):
+            if place(j) == 0:
+                halo_wait(1, True)
+            if place(j) == chunks - 1 and not end:
+                halo_wait(1, False)
+            pool_chunk(1, place(j))
+            g_send(1, 1, place(j))
+
+        return {
+            "q": lambda j: gather_next(place(j)), "m": lambda j: normalize_next(place(j)),
+            "A": lambda j: weights.arrived(1, 0), "E": lambda j: weights.arrived(1, 1),
+            "F": lambda j: weights.arrived(1, 2), "i": ready, "e": lambda j: gate_chunk(1, place(j)), "b": branch,
+            "x": lambda j: g_relay(1, 1, place(j)), "z": lambda j: emit_last(1, place(j)),
+        }
 
     def all_sent(weights):
         weights.finish()
         for layer in range(1, layers):
             halo_sent(layer)
-            for j in range(chunks):
-                g_sent(0, layer, j)
-                g_sent(1, layer, j)
+            g_sent(0, layer)
+            g_sent(1, layer)
+
+    def run(script, weights, actions):
+        counts = {}
+        for word in script:
+            if len(word) > 1:
+                weights.word(word)
+                continue
+            j = counts.get(word, 0)
+            counts[word] = j + 1
+            if j < (1 if word in "pgoROYAEF" and word not in actions["many"] else chunks):
+                actions[word](j)
+
+    def gather_next(j):
+        g_relay(0, 1, j)
+
+    def normalize_next(j):
+        g_arrived(0, 1, j)
+        normalize(1, j)
 
     def end_program():
         weights = Weights(True)
-        order = range(len(streams))
-        for q in order:
-            if edge(q):
-                weights.own(q)
+        weights.own(0)
+        weights.own(1)
         own_h.wait()
         for j in range(chunks):
             if near(j):
                 for d in range(1, chips):
                     g_copy(0, 0, j, rank, chip_rank(d), d).start()
-        for j in range(chunks):
+
+        def offer(j):
             e_copy(j, rank, inward).start()
             if near(j):
                 for d in range(1, chips):
                     source = chip_rank(d)
                     g_copy(0, 0, j, source, sibling, 0).wait_recv()
                     e_copy(j, source, inward).start()
-            if j == min(1, chunks - 1):
-                for q in order:
-                    if streams[q][:2] == (0, 2):
-                        weights.own(q)
-        for q in order:
-            if not edge(q) and streams[q][:2] != (0, 2):
-                weights.own(q)
+
+        run(SEND, weights, {"k": offer, "many": ""})
+        for q in range(len(streams)):
+            weights.own(q)
         for layer in range(layers):
             mix_matrix(layer)
             if layer:
                 guard(lambda: zero_pad(layer, 0), row_rank == 0)
                 guard(lambda: zero_pad(layer, rows + HALO), row_rank == last_row)
-        weights.advance(sum(1 for _, d in weights.all if d == 1))
-        weights.arrived(0, 2)
-        for j in range(chunks):
+
+        def receive(j):
             t_copy(j, inward).wait_recv()
             g_send(1, 0, j)
+
+        def emit(j):
             g_relay(1, 0, j)
-            if j:
-                g_relay(0, 1, j - 1)
             g_arrived(1, 0, j)
             out_chunk(0, j)
             g_send(0, 1, j)
-            if j:
-                g_arrived(0, 1, j - 1)
-                normalize(1, j - 1)
-        later_layers(weights, chunks - 1)
+
+        run(END, weights, {
+            "t": receive, "o": emit, "Y": lambda j: weights.arrived(0, 2), "many": "o",
+            **second_layer(weights, True),
+        })
+        later_layers(weights)
         all_sent(weights)
-        for j in range(chunks):
-            g_sent(1, 0, j)
-            e_copy(j, rank, inward).wait_send()
-            if near(j):
-                for d in range(1, chips):
-                    g_copy(0, 0, j, rank, chip_rank(d), d).wait_send()
-                    e_copy(j, chip_rank(d), inward).wait_send()
+        g_sent(1, 0)
+        flushed(hg.at[0, rank], es.at[rank])
+        for d in range(1, chips):
+            flushed(hg.at[0, rank], gs.at[0, d], few)
+            flushed(hg.at[0, rank], es.at[chip_rank(d)], few)
 
     def mid_program():
         weights = Weights(False)
+        weights.own(0)
+        weights.own(1)
         own_h.wait()
-        for q in range(1 + AHEAD):
-            weights.own(q)
         for j in range(chunks):
             g_send(0, 0, j)
-        for q in range(len(streams)):
-            if not edge(q):
-                weights.own(q, True)
+        for letter in EARLY:
+            weights.own(streams.index(names[letter]), True)
         for layer in range(layers):
             mix_matrix(layer)
         guard(lambda: zero_pad(0, 0), row_rank == 1)
         guard(lambda: zero_pad(0, 2 * rows + HALO), row_rank == last_row - 1)
-        entry = len([1 for q, _ in weights.all if edge(q)])
-        for j in range(chunks):
-            g_relay(0, 0, j)
-            weights.advance(entry * (j + 1) // (chunks + 1))
-            if j:
-                g_arrived(0, 0, j - 1)
-                normalize(0, j - 1)
-        g_arrived(0, 0, chunks - 1)
-        normalize(0, chunks - 1)
-        guard(lambda: host_take(0), host)
-        guard(lambda: host_relay(0), host)
-        own_project(weights, 0, own_shift)
-        weights.arrived(0, 1)
-        project(acc_g, wg, 0)
-
-        def own_pool():
-            halo_arrived(0)
-            for j in range(chunks):
-                pool_chunk(0, j)
-                g_send(1, 0, j)
-
-        def own_out():
-            for j in range(chunks):
-                g_relay(1, 0, j)
-            weights.arrived(0, 2)
-            for j in range(chunks):
-                g_arrived(1, 0, j)
-                out_chunk(0, j)
-                g_send(0, 1, j)
-
-        tail = [q for q, d in weights.all if not edge(q)]
-        for j in range(chunks):
-            if j:
-                guard(lambda: host_take(j), host)
-                guard(lambda: host_relay(j), host)
+
+        def normalize_own(j):
+            g_arrived(0, 0, j)
+            normalize(0, j)
+
+        def gate(j):
+            weights.arrived(0, 1)
+            project(acc_g, wg, 0)
+
+        def hosted(j):
+            guard(lambda: host_relay(j), host)
             guard(lambda: host_arrived(j), host)
             guard(lambda: host_project(j), host)
             if j:
                 guard(lambda: pool_hosted(j - 1), host)
-            else:
-                own_pool()
-            if j == min(OUT_AFTER, chunks - 1):
-                own_out()
-            if j > OUT_AFTER:
-                weights.upto(1, 0, 1 if j == OUT_AFTER + 1 else None)
-        guard(lambda: pool_hosted(chunks - 1), host)
-        later_layers(weights, 0)
+            if j == chunks - 1:
+                guard(lambda: pool_hosted(j), host)
+
+        def own_pool(j):
+            for i in reversed(range(chunks)):
+                if i == 0:
+                    halo_arrived(0)
+                pool_chunk(0, i)
+                g_send(1, 0, i)
+
+        def relay_branch(j):
+            for i in reversed(range(chunks)):
+                g_relay(1, 0, i)
+
+        def own_out(j):
+            weights.arrived(0, 2)
+            for i in reversed(range(chunks)):
+                g_arrived(1, 0, i)
+                out_chunk(0, i)
+                g_send(0, 1, i)
+
+        run(MID, weights, {
+            "r": lambda j: g_relay(0, 0, j), "n": normalize_own, "k": lambda j: guard(lambda: host_take(j), host),
+            "p": lambda j: own_project(weights, 0, own_shift), "g": gate, "h": hosted, "o": own_pool,
+            "R": relay_branch, "O": own_out, "many": "", **second_layer(weights, False),
+        })
+        later_layers(weights)
         all_sent(weights)
         halo_sent(0)
-        for j in range(chunks):
-            g_sent(0, 0, j)
-            g_sent(1, 0, j)
-            guard(lambda: host_sent(j), host)
+        g_sent(0, 0)
+        g_sent(1, 0)
+        guard(host_sent, host)
 
     pl.when(at_end)(end_program)
     pl.when(jnp.logical_not(at_end))(mid_program)
+    for j in range(chunks):
+        o_copy(j).wait()
 
 
 def solution(mesh):
@@ -634,7 +727,7 @@
             functools.partial(mixer, dims),
             out_shape=jax.ShapeDtypeStruct((rows, cols), bf16),
             in_specs=[hbm, vmem, hbm, hbm, vmem, hbm],
-            out_specs=vmem,
+            out_specs=hbm,
             scratch_shapes=[
                 pltpu.VMEM((layers, tp_size, rows, cols), bf16),
                 pltpu.VMEM((tp_size, rows, cols), bf16),
@@ -651,17 +744,18 @@
                 pltpu.VMEM((rows, chans), f32),
                 pltpu.VMEM((layers, chans, chans), bf16),
                 dma((1 + 3 * layers,)),
+                dma((chunks,)),
                 dma((streams, sp_size)),
                 dma((streams, sp_size + 1)),
                 dma((3 * layers, sp_size)),
                 dma((3 * layers, sp_size)),
                 dma((2 * layers * chunks, tp_size)),
-                dma((2 * layers * chunks, tp_size)),
+                dma((2 * layers, tp_size)),
                 dma((chunks, tp_size)),
-                dma((chunks, tp_size)),
-                dma((chunks, tp_size)),
+                dma((tp_size,)),
+                dma((tp_size,)),
                 dma((chunks,)),
-                dma((chunks,)),
+                dma((1,)),
                 dma((layers, 2)),
                 dma((layers, 2)),
             ],

time: 213 us -> 116 us (0.54)
  Pallas kernels: 210 us -> 113 us
    pallas_call x1, Pallas kernels: 210 us -> 113 us  [local(): pl.pallas_call(functools.partial(mixer, dims), out_shape=jax.ShapeDtypeSt...]
where the time goes in v2:
time: 116 us
  Pallas kernels  113 us (97%)
  local copies, waits for them, and re-layouts  2.47 us (2%)
    pallas_call x1, Pallas kernels, local(): pl.pallas_call(functools.partial(mixer, dims), out_shape=jax.ShapeDtypeSt...  113 us
    unnamed x1, local copies, waits for them, and re-layouts  2.47 us

profile of v2, /device:TPU:0, one launch (start us, length us, event | category | flops | bytes accessed | tf_op | source)
XLA Modules:
  0.0 115.6 jit_solution(15803631822620789235)
XLA Ops:
  0.0 113.1 %shard_map.64 = bf16[640,1024]{1,0:T(8,128)(2,1)} custom-call(bf16[640,1024]{1,0:T(8,128)(2,1)} %h_in.1, f32[2,4096]{1,0:T(2,128)} %gain.1, bf16[2,1024,256]{2,1,0:T(8,128)(2,1)} %w_in.1, bf16[2,1024,256]{2,1,0:T(8,128)(2,1)} %w_gate.1, bf16[2,16,64,64]{3,2,1,0:T(8,128)(2,1)} %mix.1, bf16[2,256,1024]{2,1,0:T(8,128)(2,1)} %w_out.1), custom_call_target="tpu_custom_call" | custom-call | tf_op jit(solution)/shard_map/pallas_call | solution.py:726
  113.1 2.5 %copy.8 = bf16[640,1024]{1,0:T(8,128)(2,1)} copy(bf16[640,1024]{1,0:T(8,128)(2,1)} %shard_map.64) | data formatting | bytes 2621440

commit v3 on v2

--- a/solution.py
+++ b/solution.py
@@ -13,8 +13,8 @@
 NEAR = (4,)
 SEND = ('k', 'cs', 'k', 'k', 'k', 'ds', 'k', 'es', 'fs', 'ps', 'qs', 'rs')
 EARLY = "cdef"
-MID = ('ao', 'ai1', 'r', 'bo', 'bi1', 'xs', 'cs', 'r', 'n', 'ai', 'k', 'r', 'n', 'bi', 'co', 'r', 'n', 'k', 'xi', 'r', 'n', 'ci1', 'k', 'n', 'p', 'ds', 'g', 'ci', 'es', 'k', 'h', 'h', 'di1', 'o', 'h', 'do', 'h', 'fs', 'k', 'ei1', 'h', 'R', 'O', 'di', 'eo', 'fo', 'q', 'm', 'ei', 'fi1', 'q', 'm', 'fi', 'po', 'A', 'i', 'i', 'q', 'm', 'qo', 'i', 'E', 'e', 'e', 'e', 'q', 'm', 'i', 'e', 'b', 'b', 'b', 'ro', 'q', 'm', 'i', 'e', 'b', 'b', 'x', 'x', 'x', 'x', 'x', 'F', 'z', 'z', 'z', 'z', 'z')
-END = ('ci1', 'di1', 'ei1', 'fi1', 'ci2', 'ci', 't', 't', 'Y', 'o', 'di2', 't', 'o', 't', 't', 'o', 'ei2', 'o', 'di', 'o', 'q', 'm', 'q', 'm', 'ei', 'q', 'm', 'A', 'i', 'i', 'i', 'fi2', 'q', 'm', 'i', 'E', 'e', 'e', 'b', 'e', 'b', 'fi', 'e', 'b', 'q', 'm', 'i', 'e', 'b', 'x', 'x', 'b', 'x', 'x', 'x', 'F', 'z', 'z', 'z', 'z', 'z')
+MID = ('ao', 'ai1', 'r', 'bo', 'bi1', 'xs', 'cs', 'r', 'n', 'ai', 'k', 'r', 'n', 'bi', 'co', 'r', 'n', 'k', 'xi', 'r', 'n', 'ci1', 'k', 'n', 'p', 'ds', 'g', 'ci', 'es', 'k', 'h', 'h', 'di1', 'o', 'h', 'do', 'h', 'fs', 'ei1', 'R', 'O', 'k', 'h', 'di', 'eo', 'fo', 'q', 'm', 'ei', 'fi1', 'q', 'm', 'fi', 'po', 'A', 'i', 'i', 'q', 'm', 'qo', 'i', 'E', 'e', 'q', 'm', 'i', 'e', 'b', 'b', 'b', 'ro', 'q', 'm', 'i', 'e', 'b', 'b', 'x', 'x', 'x', 'x', 'F', 'z', 'z', 'x', 'z', 'z', 'z')
+END = ('ci1', 'di1', 'ei1', 'fi1', 'ci2', 'ci', 't', 't', 'Y', 'o', 'di2', 't', 'o', 't', 't', 'o', 'ei2', 'o', 'di', 'o', 'q', 'm', 'q', 'm', 'ei', 'q', 'm', 'A', 'i', 'i', 'i', 'fi2', 'q', 'm', 'i', 'E', 'e', 'e', 'fi', 'b', 'b', 'b', 'q', 'm', 'i', 'e', 'b', 'b', 'x', 'x', 'x', 'x', 'F', 'z', 'z', 'x', 'z', 'z', 'z')
 MESH = pl.DeviceIdType.MESH
 
 norm_eps = 1e-06
@@ -34,7 +34,7 @@
         pl.when(traced)(body)
 
 
-def mixer(dims, h_in, gain, w_in, w_gate, mix, w_out, out, hg, hh, nb, nh, br, bh, wi, wg, wo, pad, acc_p, acc_g,
+def mixer(dims, h_in, gain_in, w_in, w_gate, mix_in, w_out, out, gain, mix, hg, hh, nb, nh, br, bh, wi, wg, wo, pad, acc_p, acc_g,
           gate_h, bd, local_sem, out_sem, zr, zs, yr, ys, gr, gs, er, es, hs, tr, ts, pr, ps):
     sp_size, tp_size, layers, rows, cols, chans, chunks = dims
     step_rows = rows // chunks
@@ -82,6 +82,11 @@
     own_h = pltpu.make_async_copy(h_in, hg.at[0, rank], local_sem.at[0])
     own_h.start()
 
+    own_gain = pltpu.make_async_copy(gain_in, gain, local_sem.at[1 + 3 * layers])
+    own_mix = pltpu.make_async_copy(mix_in, mix, local_sem.at[2 + 3 * layers])
+    own_gain.start()
+    own_mix.start()
+
     barrier = pltpu.get_barrier_semaphore()
     peers = [
         {"sp": lax.rem(row_rank + 1, sp_size)},
@@ -206,8 +211,8 @@
         scaling = lax.rsqrt(squares / (cols * tp_size) + norm_eps)
         for k in range(tp_size):
             block = source[k, at, :].astype(jnp.float32)
-            own_gain = gain[layer : layer + 1, k * cols : (k + 1) * cols]
-            target[k, to, :] = (block * scaling * own_gain).astype(jnp.bfloat16)
+            scale = gain[layer : layer + 1, k * cols : (k + 1) * cols]
+            target[k, to, :] = (block * scaling * scale).astype(jnp.bfloat16)
 
     def normalize(layer, j):
         scaled(hg.at[layer], span(j), nb, span(j), layer)
@@ -504,8 +509,12 @@
         rounded = project_chunk(wi, layer, j).astype(jnp.bfloat16).astype(jnp.float32)
         pad[layer, pl.ds(aligned(HALO + first(j)), step_rows), :] = rounded
 
-    def gate_chunk(layer, j):
-        acc_g[span(j), :] = project_chunk(wg, layer, j)
+    def gate_rows(layer, at, count):
+        total = jnp.zeros((count, chans), jnp.float32)
+        for k in range(tp_size):
+            weight = wg[layer, k * cols : (k + 1) * cols, :]
+            total = total + jnp.dot(nb[k, at, :], weight, preferred_element_type=jnp.float32)
+        acc_g[at, :] = total
 
     def own_project(weights, layer, shift):
         weights.arrived(layer, 0)
@@ -534,7 +543,7 @@
             weights.arrived(layer, 1)
             halo_arrived(layer)
             for j in range(chunks):
-                gate_chunk(layer, j)
+                gate_rows(layer, span(j), step_rows)
                 pool_chunk(layer, j)
                 g_send(1, layer, j)
             for j in range(chunks):
@@ -554,6 +563,13 @@
             if place(j) == chunks - 1:
                 halo_side(1, False)
 
+        def gate_pair(j):
+            if 2 * j + 1 < chunks:
+                begin = jnp.minimum(first(place(2 * j)), first(place(2 * j + 1)))
+                gate_rows(1, pl.ds(pl.multiple_of(begin, step_rows), 2 * step_rows), 2 * step_rows)
+            elif 2 * j < chunks:
+                gate_rows(1, span(place(2 * j)), step_rows)
+
         def branch(j):
             if place(j) == 0:
                 halo_wait(1, True)
@@ -565,7 +581,7 @@
         return {
             "q": lambda j: gather_next(place(j)), "m": lambda j: normalize_next(place(j)),
             "A": lambda j: weights.arrived(1, 0), "E": lambda j: weights.arrived(1, 1),
-            "F": lambda j: weights.arrived(1, 2), "i": ready, "e": lambda j: gate_chunk(1, place(j)), "b": branch,
+            "F": lambda j: weights.arrived(1, 2), "i": ready, "e": gate_pair, "b": branch,
             "x": lambda j: g_relay(1, 1, place(j)), "z": lambda j: emit_last(1, place(j)),
         }
 
@@ -615,6 +631,8 @@
         run(SEND, weights, {"k": offer, "many": ""})
         for q in range(len(streams)):
             weights.own(q)
+        own_gain.wait()
+        own_mix.wait()
         for layer in range(layers):
             mix_matrix(layer)
             if layer:
@@ -652,6 +670,8 @@
             g_send(0, 0, j)
         for letter in EARLY:
             weights.own(streams.index(names[letter]), True)
+        own_gain.wait()
+        own_mix.wait()
         for layer in range(layers):
             mix_matrix(layer)
         guard(lambda: zero_pad(0, 0), row_rank == 1)
@@ -722,13 +742,15 @@
         dims = (sp_size, tp_size, layers, rows, cols, chans, chunks)
         bf16, f32 = jnp.bfloat16, jnp.float32
         dma = pltpu.SemaphoreType.DMA
-        hbm, vmem = pl.BlockSpec(memory_space=pl.ANY), pl.BlockSpec(memory_space=pltpu.VMEM)
+        hbm = pl.BlockSpec(memory_space=pl.ANY)
         return pl.pallas_call(
             functools.partial(mixer, dims),
             out_shape=jax.ShapeDtypeStruct((rows, cols), bf16),
-            in_specs=[hbm, vmem, hbm, hbm, vmem, hbm],
+            in_specs=[hbm] * 6,
             out_specs=hbm,
             scratch_shapes=[
+                pltpu.VMEM(norm_gain.shape, f32),
+                pltpu.VMEM(group_mix.shape, bf16),
                 pltpu.VMEM((layers, tp_size, rows, cols), bf16),
                 pltpu.VMEM((tp_size, rows, cols), bf16),
                 pltpu.VMEM((tp_size, rows, cols), bf16),
@@ -743,7 +765,7 @@
                 pltpu.VMEM((rows, chans), f32),
                 pltpu.VMEM((rows, chans), f32),
                 pltpu.VMEM((layers, chans, chans), bf16),
-                dma((1 + 3 * layers,)),
+                dma((3 + 3 * layers,)),
                 dma((chunks,)),
                 dma((streams, sp_size)),
                 dma((streams, sp_size + 1)),

time: 116 us -> 114 us (0.983)
    pallas_call x1, Pallas kernels: 113 us -> 112 us  [local(): pl.pallas_call(functools.partial(mixer, dims), out_shape=jax.ShapeDtypeSt...]
where the time goes in v3:
time: 114 us
  Pallas kernels  112 us (98%)
  local copies, waits for them, and re-layouts  2.47 us (2%)
    pallas_call x1, Pallas kernels, local(): pl.pallas_call(functools.partial(mixer, dims), out_shape=jax.ShapeDtypeSt...  112 us
    unnamed x1, local copies, waits for them, and re-layouts  2.47 us

profile of v3, /device:TPU:0, one launch (start us, length us, event | category | flops | bytes accessed | tf_op | source)
XLA Modules:
  0.0 114.1 jit_solution(14233719889060277164)
XLA Ops:
  0.0 111.7 %shard_map.64 = bf16[640,1024]{1,0:T(8,128)(2,1)} custom-call(bf16[640,1024]{1,0:T(8,128)(2,1)} %h_in.1, f32[2,4096]{1,0:T(2,128)} %gain_in.1, bf16[2,1024,256]{2,1,0:T(8,128)(2,1)} %w_in.1, bf16[2,1024,256]{2,1,0:T(8,128)(2,1)} %w_gate.1, bf16[2,16,64,64]{3,2,1,0:T(8,128)(2,1)} %mix_in.1, bf16[2,256,1024]{2,1,0:T(8,128)(2,1)} %w_out.1), custom_call_target="tpu_custom_call" | custom-call | tf_op jit(solution)/shard_map/pallas_call | solution.py:746
  111.7 2.5 %copy.8 = bf16[640,1024]{1,0:T(8,128)(2,1)} copy(bf16[640,1024]{1,0:T(8,128)(2,1)} %shard_map.64) | data formatting | bytes 2621440

commit v4 on v3

--- a/solution.py
+++ b/solution.py
@@ -138,13 +138,13 @@
         layer, t, kind = streams[q]
         ref = piece_ref(layer, t, source, half if kind == "main" else other)
         return pltpu.make_async_remote_copy(
-            ref, ref, zs.at[q, send], zr.at[q, source], device_id={"sp": to}, device_id_type=MESH
+            ref, ref, zs.at[q], zr.at[q, source], device_id={"sp": to}, device_id_type=MESH
         )
 
     def y_copy(layer, t, source, part):
         ref = piece_ref(layer, t, source, part)
         return pltpu.make_async_remote_copy(
-            ref, ref, ys.at[layer * 3 + t, source], yr.at[layer * 3 + t, source],
+            ref, ref, ys.at[layer * 3 + t], yr.at[layer * 3 + t, source],
             device_id={"grp": other}, device_id_type=MESH,
         )
 
@@ -346,13 +346,6 @@
                 row_rank != source, swapped(layer, t, source, end),
             )
 
-    def y_sent(layer, t, end):
-        for source in range(sp_size):
-            guard(
-                lambda source=source: y_copy(layer, t, source, half).wait_send(),
-                row_rank != source, swapped(layer, t, source, end),
-            )
-
     names = {letter: (i // 3, i % 3, "main") for i, letter in enumerate("abcdef")}
     names.update(p=(1, 0, "near"), q=(1, 1, "near"), r=(1, 2, "near"), x=(0, 0, "core"), y=(0, 1, "core"), w=(0, 2, "inner"), v=(1, 0, "core"), u=(1, 1, "core"))
 
@@ -444,27 +437,35 @@
             y_wait(layer, t, self.end)
 
         def finish(self):
+            inside = False if host is True else jnp.logical_not(host)
             for q, (layer, t, kind) in enumerate(streams):
-                low, high = limits(q)
+                shard, whole = shards[t]
+
+                def flush(sem, count, *conditions, layer=layer, whole=whole, size=shard.shape[1] // 2):
+                    part = whole.at[layer, pl.ds(0, count * size)]
+                    guard(lambda: pltpu.make_async_remote_copy(
+                        part, part, sem, zr.at[0, 0], device_id={"tp": sibling}, device_id_type=MESH
+                    ).wait_send(), *conditions)
+
+                swap = ys.at[layer * 3 + t]
+                kinds = FULL.get((layer, t), ())
                 if self.end:
-                    included = member(kind, row_rank)
-                    guard(lambda: z_copy(q, row_rank, up, row_rank).wait_send(), included, row_rank == 0)
-                    guard(lambda: z_copy(q, row_rank, down, sp_size).wait_send(), included, row_rank == last_row)
-                elif kind != "near":
-                    for source in range(sp_size):
-                        included = member(kind, source)
-
-                        def sent(source=source):
-                            z_copy(q, source, up, source).wait_send()
-
-                        guard(sent, included, source <= row_rank, row_rank + 1 <= high)
-                        guard(sent, included, source > row_rank, row_rank - 1 >= low)
-                    guard(
-                        lambda: z_copy(q, row_rank, down, sp_size).wait_send(),
-                        member(kind, row_rank), row_rank - 1 >= low,
-                    )
-                if kind == "main" and not (self.end and edge(q)):
-                    y_sent(layer, t, self.end)
+                    if kind != "core":
+                        flush(zs.at[q], 1)
+                    if kind == "main" and not edge(q):
+                        flush(swap, sp_size - 1)
+                    continue
+                if kind == "core":
+                    flush(zs.at[q], 1, host)
+                    flush(zs.at[q], sp_size - 1, inside)
+                elif kind == "main":
+                    flush(zs.at[q], 2 if edge(q) else sp_size + 1, host)
+                    flush(zs.at[q], sp_size + 1, inside)
+                    if "core" in kinds:
+                        flush(swap, 2)
+                    else:
+                        flush(swap, sp_size - 2 if "near" in kinds else sp_size - 1, host)
+                        flush(swap, sp_size - 1, inside)
 
     def host_take(j):
         e_copy(j, rank, outward).wait_recv()
@@ -768,9 +769,9 @@
                 dma((3 + 3 * layers,)),
                 dma((chunks,)),
                 dma((streams, sp_size)),
-                dma((streams, sp_size + 1)),
+                dma((streams,)),
                 dma((3 * layers, sp_size)),
-                dma((3 * layers, sp_size)),
+                dma((3 * layers,)),
                 dma((2 * layers * chunks, tp_size)),
                 dma((2 * layers, tp_size)),
                 dma((chunks, tp_size)),

time: 114 us -> 114 us (level)
  no operation moved by 1% of the time
where the time goes in v4:
time: 114 us
  Pallas kernels  111 us (97%)
  local copies, waits for them, and re-layouts  2.47 us (2%)
    pallas_call x1, Pallas kernels, local(): pl.pallas_call(functools.partial(mixer, dims), out_shape=jax.ShapeDtypeSt...  111 us
    unnamed x1, local copies, waits for them, and re-layouts  2.47 us

profile of v4, /device:TPU:0, one launch (start us, length us, event | category | flops | bytes accessed | tf_op | source)
XLA Modules:
  0.0 113.6 jit_solution(1063757168836934694)
XLA Ops:
  0.0 111.1 %shard_map.64 = bf16[640,1024]{1,0:T(8,128)(2,1)} custom-call(bf16[640,1024]{1,0:T(8,128)(2,1)} %h_in.1, f32[2,4096]{1,0:T(2,128)} %gain_in.1, bf16[2,1024,256]{2,1,0:T(8,128)(2,1)} %w_in.1, bf16[2,1024,256]{2,1,0:T(8,128)(2,1)} %w_gate.1, bf16[2,16,64,64]{3,2,1,0:T(8,128)(2,1)} %mix_in.1, bf16[2,256,1024]{2,1,0:T(8,128)(2,1)} %w_out.1), custom_call_target="tpu_custom_call" | custom-call | tf_op jit(solution)/shard_map/pallas_call | solution.py:747
  111.1 2.5 %copy.8 = bf16[640,1024]{1,0:T(8,128)(2,1)} copy(bf16[640,1024]{1,0:T(8,128)(2,1)} %shard_map.64) | data formatting | bytes 2621440
